TPU v7x, 32 devices: a whole 2x2x4 slice. The times are simulated.
32 devices in a mesh: ep: 8 (over z, x), tp: 4 (over y, core).
Axes of the slice: x: 2, y: 2, z: 4, core: 2. Of those that a mesh axis runs over, the one named last changes fastest.
Arguments:
- q_in: bfloat16 [4096, 1024], P('ep', 'tp'), may hold values from -6 to 6
- k_in: bfloat16 [4096, 256], P('ep'), may hold values from -6 to 6
- v_in: bfloat16 [4096, 256], P('ep'), may hold values from -6 to 6
- q_gain: float32 [64], replicated, may hold values from 0.1 to 1.9
- k_gain: float32 [64], replicated, may hold values from 0.1 to 1.9
- w_out: bfloat16 [1024, 2048], P('tp'), may hold values from -0.1875 to 0.1875
- post_gain: float32 [2048], replicated, may hold values from 0.1 to 1.9
- moe_in: bfloat16 [1024, 2048], P('ep'), may hold values from -6 to 6
- routes: int32 [1024, 2], P('ep'), may hold values from 0 to 7, all different within a row; in each aligned block of 128 rows (0 to 127, 128 to 255, ...) at most 48 rows name the same one
- route_logits: float32 [1024, 2], P('ep'), may hold values from -6 to 6
- pre_gain: float32 [2048], replicated, may hold values from 0.1 to 1.9
- w_gate: bfloat16 [8, 2048, 4096], P('ep', None, 'tp'), may hold values from -0.125 to 0.125
- w_up: bfloat16 [8, 2048, 4096], P('ep', None, 'tp'), may hold values from -0.125 to 0.125
- w_down: bfloat16 [8, 4096, 2048], P('ep', 'tp'), may hold values from -0.125 to 0.125
Outputs:
- attn_out: bfloat16 [4096, 2048], P(('ep', 'tp'))
- moe_out: bfloat16 [1024, 2048], P('ep', 'tp')
Inputs may be any that keep to these rules, and one draw needn't show every extreme that they name: `routes`: each row names 2 different experts. Among the rows of one index of ep no expert is named by more than 48 rows, a bound that some block reaches of them.
All inputs are finite; a program needn't handle non-finite values.
Results may differ from a plain program's by a relative error of at most 0.018.
Values may be sent and summed in bfloat16 or wider, within the bound.
A program may use at most 64 MiB of HBM per device.

v0:
```python
import jax
import jax.numpy as jnp
from jax import lax
from jax.sharding import PartitionSpec as P

GRID_W = 128
EPSILON = 1e-06
ROPE_BASE = 10000.0


def head_norm(values, gain):
    return values * lax.rsqrt(jnp.mean(values * values, axis=-1, keepdims=True) + EPSILON) * gain


def rotate_half(values, angles):
    quarter = angles.shape[-1]
    first_part = values[..., :quarter]
    second_part = values[..., quarter:]
    cosine = jnp.cos(angles)[:, None, :]
    sine_part = jnp.sin(angles)[:, None, :]
    return jnp.concatenate(
        [
            first_part * cosine - second_part * sine_part,
            second_part * cosine + first_part * sine_part,
        ],
        axis=-1,
    )


def grid_rotary(values, offset):
    row_count = values.shape[0]
    head_width = values.shape[-1]
    quarter = head_width // 4
    half_width = head_width // 2
    position = offset + jnp.arange(row_count, dtype=jnp.int32)
    grid_row = (position // GRID_W).astype(jnp.float32)
    grid_col = (position % GRID_W).astype(jnp.float32)
    inverse = ROPE_BASE ** (-jnp.arange(quarter, dtype=jnp.float32) / quarter)
    return jnp.concatenate(
        [
            rotate_half(values[..., :half_width], grid_row[:, None] * inverse[None, :]),
            rotate_half(values[..., half_width:], grid_col[:, None] * inverse[None, :]),
        ],
        axis=-1,
    )


def slot_table(route_rows, expert_count, capacity):
    token_count, top_count = route_rows.shape
    flat_routes = route_rows.reshape(-1)
    one_hot = (flat_routes[:, None] == jnp.arange(expert_count, dtype=jnp.int32)[None, :]).astype(
        jnp.int32
    )
    ranked = jnp.sum((jnp.cumsum(one_hot, axis=0) - 1) * one_hot, axis=1)
    placed = flat_routes * capacity + ranked
    slot_owner = jnp.full((expert_count * capacity,), token_count * top_count, dtype=jnp.int32)
    slot_owner = slot_owner.at[placed].set(jnp.arange(token_count * top_count, dtype=jnp.int32))
    return (slot_owner, placed)


def mixer_half(q_in, k_in, v_in, q_gain, k_gain, w_out, post_gain):
    head_size = q_gain.shape[0]
    row_count = q_in.shape[0]
    local_heads = q_in.shape[1] // head_size
    kv_count = k_in.shape[1] // head_size
    tp_count = lax.axis_size("tp")
    repeat = local_heads * tp_count // kv_count
    offset = lax.axis_index("ep") * row_count
    queries = head_norm(q_in.astype(jnp.float32).reshape(row_count, local_heads, head_size), q_gain)
    queries = grid_rotary(queries, offset).astype(jnp.bfloat16)
    query_rows = jnp.transpose(queries, (1, 0, 2)).reshape(local_heads * row_count, head_size)
    kv_index = lax.axis_index("tp") * local_heads // repeat
    own_keys = lax.dynamic_slice_in_dim(k_in, kv_index * head_size, head_size, 1)
    own_values = lax.dynamic_slice_in_dim(v_in, kv_index * head_size, head_size, 1)
    own_keys = head_norm(own_keys.astype(jnp.float32)[:, None, :], k_gain)
    own_keys = grid_rotary(own_keys, offset)[:, 0, :].astype(jnp.bfloat16)
    paired = jnp.concatenate([own_keys, own_values], axis=1)
    scale_factor = head_size ** (-0.5)

    def attend_block(running, key_block):
        block_keys = key_block[:, :head_size]
        block_values = key_block[:, head_size:]
        scores = (
            jnp.einsum("qd,kd->qk", query_rows, block_keys, preferred_element_type=jnp.float32)
            * scale_factor
        )
        weights = jnp.exp(scores)
        numer = running[0] + jnp.dot(
            weights.astype(jnp.bfloat16), block_values, preferred_element_type=jnp.float32
        )
        return (numer, running[1] + jnp.sum(weights, axis=1))

    zero_init = (
        jnp.zeros((local_heads * row_count, head_size), jnp.float32),
        jnp.zeros((local_heads * row_count,), jnp.float32),
    )
    running = zero_init
    gathered_piece = lax.all_gather(paired, "ep", axis=0, tiled=True)
    piece_rows = gathered_piece.shape[0]
    blocks = gathered_piece.reshape(piece_rows // 512, 512, gathered_piece.shape[1])

    def scan_block(partial_value, key_block):
        return (attend_block(partial_value, key_block), None)

    running, unused = lax.scan(scan_block, running, blocks)
    numer, denom = running
    head_out = (numer / denom[:, None]).astype(jnp.bfloat16)
    head_out = jnp.transpose(head_out.reshape(local_heads, row_count, head_size), (1, 0, 2))
    head_out = head_out.reshape(row_count, local_heads * head_size)
    mixed = lax.psum_scatter(
        jnp.dot(head_out, w_out, preferred_element_type=jnp.float32).astype(jnp.bfloat16),
        "tp",
        scatter_dimension=0,
        tiled=True,
    ).astype(jnp.float32)
    return head_norm(mixed, post_gain).astype(jnp.bfloat16)


def experts_half(moe_in, routes, route_logits, pre_gain, w_gate, w_up, w_down):
    token_count, top_count = routes.shape
    model_width = moe_in.shape[1]
    expert_count = lax.axis_size("ep")
    capacity = max(2, 3 * top_count * token_count // (2 * expert_count))
    tp_count = lax.axis_size("tp")
    slice_width = model_width // tp_count
    normed = head_norm(moe_in.astype(jnp.float32), pre_gain).astype(jnp.bfloat16)
    slot_owner, placed = slot_table(routes, expert_count, capacity)
    padded = jnp.concatenate([normed, jnp.zeros((1, model_width), jnp.bfloat16)], axis=0)
    outgoing = padded[slot_owner // top_count].reshape(expert_count, capacity, model_width)
    arrived = lax.all_to_all(outgoing, "ep", split_axis=0, concat_axis=0, tiled=True)
    arrived = arrived.reshape(expert_count * capacity, model_width)
    gate_pre = jnp.dot(arrived, w_gate[0], preferred_element_type=jnp.float32)
    up_pre = jnp.dot(arrived, w_up[0], preferred_element_type=jnp.float32)
    hidden = (jax.nn.silu(gate_pre) * up_pre).astype(jnp.bfloat16)
    partial_out = jnp.dot(hidden, w_down[0], preferred_element_type=jnp.float32)
    partial_out = partial_out.reshape(expert_count, capacity, model_width)
    summed = lax.psum_scatter(
        partial_out.astype(jnp.bfloat16), "tp", scatter_dimension=2, tiled=True
    )
    returned = lax.all_to_all(summed, "ep", split_axis=0, concat_axis=0, tiled=True)
    returned = returned.reshape(expert_count * capacity, slice_width)
    copies = returned[placed].reshape(token_count, top_count, slice_width).astype(jnp.float32)
    route_weight = jax.nn.softmax(route_logits, axis=-1)
    return jnp.sum(route_weight[..., None] * copies, axis=1).astype(jnp.bfloat16)


def per_device(
    q_in,
    k_in,
    v_in,
    q_gain,
    k_gain,
    w_out,
    post_gain,
    moe_in,
    routes,
    route_logits,
    pre_gain,
    w_gate,
    w_up,
    w_down,
):
    attn_out = mixer_half(q_in, k_in, v_in, q_gain, k_gain, w_out, post_gain)
    moe_out = experts_half(moe_in, routes, route_logits, pre_gain, w_gate, w_up, w_down)
    return (attn_out, moe_out)


def solution(mesh):
    return jax.shard_map(
        per_device,
        mesh=mesh,
        in_specs=(
            P("ep", "tp"),
            P("ep", None),
            P("ep", None),
            P(),
            P(),
            P("tp", None),
            P(),
            P("ep", None),
            P("ep", None),
            P("ep", None),
            P(),
            P("ep", None, "tp"),
            P("ep", None, "tp"),
            P("ep", "tp", None),
        ),
        out_specs=(P(("ep", "tp"), None), P("ep", "tp")),
        check_vma=False,
    )
```

profile of v0, /device:TPU:0, one launch (start us, length us, event | category | flops | bytes accessed | tf_op | source)
XLA Modules:
  0.0 186.0 jit_solution(11214696343545034479)
XLA Ops:
  8.0 0.9 copy.40
  9.2 0.7 broadcast_multiply_fusion
  9.9 0.6 reduce-window.6
  10.4 0.2 slice_reduce_fusion
  10.8 0.1 mul.344
  11.1 1.4 scatter_custom_fusion
  12.5 1.2 fusion.22
  13.7 1.2 fusion.24
  15.0 3.1 %gather_fusion = bf16[384,2048]{1,0:T(8,128)(2,1)} fusion(bf16[129,2048]{1,0:T(8,128)(2,1)S(1)} %concatenate.17, s32[1024]{0:T(1024)S(1)} %pad_clamp_fusion.1), kind=kCustom, calls=%fused_computation | custom fusion | bytes 3147264 | tf_op jit(solution)/shard_map/gather | solution.py:129
  18.2 7.4 %all-to-all-start = ((bf16[8,48,2048]{2,1,0:T(8,128)(2,1)}), bf16[8,48,2048]{2,1,0:T(8,128)(2,1)}, u32[]{:S(2)}, u32[]{:S(2)}) async-start(bf16[8,48,2048]{2,1,0:T(8,128)(2,1)} %bitcast.13), calls=%async_computation.1 | async-start | bytes 3145728 | tf_op jit(solution)/shard_map/all_to_all | solution.py:130
  25.7 0.1 constant_dynamic-slice_fusion
  26.2 0.3 fusion.43
  26.6 0.7 pad_maximum_fusion
  27.3 0.1 copy.33
  27.6 0.3 multiply_cosine_fusion.1
  28.1 0.3 copy.43
  28.4 50.5 %all-gather.2.cloned.1.call-done = bf16[4096,128]{0,1:T(8,128)(2,1)} async-done(((bf16[512,128]{0,1:T(8,128)(2,1)}), bf16[4096,128]{0,1:T(8,128)(2,1)}) %all-gather.2.cloned.1.call-update) | async-done | bytes 1048592 | tf_op jit(solution)/shard_map/all_gather | solution.py:98
  78.9 1.6 copy.42
  80.6 4.6 %fusion.12 = f32[384,1024]{1,0:T(8,128)S(1)} fusion(bf16[384,2048]{1,0:T(8,128)(2,1)} %bitcast.14, bf16[1,2048,1024]{2,1,0:T(8,128)(2,1)} %param.27), kind=kOutput, calls=%fused_computation.18 | convolution fusion | flops 1610612736 | bytes 7340032 | tf_op jit(solution)/shard_map/dot_general | solution.py:132
  85.2 3.5 %multiply_convert_fusion = bf16[384,1024]{1,0:T(8,128)(2,1)S(1)} fusion(f32[384,1024]{1,0:T(8,128)S(1)} %fusion.12, bf16[384,2048]{1,0:T(8,128)(2,1)} %bitcast.14, bf16[1,2048,1024]{2,1,0:T(8,128)(2,1)S(1)} %copy-done.8), kind=kOutput, calls=%fused_computation.22 | convolution fusion | flops 1612972032 | bytes 8126464 | tf_op jit(solution)/shard_map/dot_general | solution.py:133
  88.8 3.0 %fusion.14 = bf16[8,48,2048]{2,1,0:T(8,128)(2,1)} fusion(bf16[8,48,1024]{2,1,0:T(8,128)(2,1)S(1)} %bitcast.62, bf16[1,1024,2048]{2,1,0:T(8,128)(2,1)S(1)} %copy-done.9), kind=kOutput, calls=%fused_computation.21 | convolution fusion | flops 1611399168 | bytes 6553600 | tf_op jit(solution)/shard_map/dot_general | solution.py:135
  91.8 46.4 %while.13 = (s32[]{:T(128)}, f32[2048,64]{0,1:T(8,128)S(1)}, f32[2048]{0:T(1024)S(1)}, bf16[8,512,128]{2,1,0:T(8,128)(2,1)S(1)}, bf16[2048,64]{1,0:T(8,128)(2,1)S(1)}, /*index=5*/s32[]{:T(128)}, s32[]{:T(128)}) while((s32[]{:T(128)}, f32[2048,64]{0,1:T(8,128)S(1)}, f32[2048]{0:T(1024)S(1)}, bf16[8,512,128]{2,1,0:T(8,128)(2,1)S(1)}, ...), condition=%wide.region_4.5_spmd.clone, body=%wide.region_2.4_spmd.clone.sunk | while | flops 272893952 | bytes 10256476 | solution.py:105
  91.9 2.7 %fusion.72 = (f32[2048]{0:T(1024)S(1)}, f32[512,2048]{1,0:T(8,128)}) fusion(bf16[2048,64]{1,0:T(8,128)(2,1)S(1)} %get-tuple-element.147, bf16[512,128]{1,0:T(8,128)(2,1)S(1)} %dynamic-slice_bitcast_fusion.2), kind=kOutput, calls=%fused_computation.4.clone.1 | convolution fusion | flops 136312832 | bytes 4595712 | tf_op jit(solution)/shard_map/while/body/eval_jaxpr/qd,kd->qk/dot_general | solution.py:84
  94.5 3.1 %convolution_add_fusion.2 = f32[2048,64]{0,1:T(8,128)S(1)} fusion(f32[512,2048]{1,0:T(8,128)} %get-tuple-element.127, f32[2048,64]{0,1:T(8,128)S(1)} %get-tuple-element.137, pred[]{:T(512)S(6)} %compare.19, bf16[512,128]{1,0:T(8,128)(2,1)S(1)} %dynamic-slice_bitcast_fusion.2), kind=kOutput, calls=%fused_computation.6.clone.1 | convolution fusion | flops 136577024 | bytes 5373953 | tf_op jit(solution)/shard_map/while/body/eval_jaxpr/dot_general | solution.py:88
  97.7 2.7 %fusion.72 = (f32[2048]{0:T(1024)S(1)}, f32[512,2048]{1,0:T(8,128)}) fusion(bf16[2048,64]{1,0:T(8,128)(2,1)S(1)} %get-tuple-element.147, bf16[512,128]{1,0:T(8,128)(2,1)S(1)} %dynamic-slice_bitcast_fusion.2), kind=kOutput, calls=%fused_computation.4.clone.1 | convolution fusion | flops 136312832 | bytes 4595712 | tf_op jit(solution)/shard_map/while/body/eval_jaxpr/qd,kd->qk/dot_general | solution.py:84
  100.3 3.2 %convolution_add_fusion.2 = f32[2048,64]{0,1:T(8,128)S(1)} fusion(f32[512,2048]{1,0:T(8,128)} %get-tuple-element.127, f32[2048,64]{0,1:T(8,128)S(1)} %get-tuple-element.137, pred[]{:T(512)S(6)} %compare.19, bf16[512,128]{1,0:T(8,128)(2,1)S(1)} %dynamic-slice_bitcast_fusion.2), kind=kOutput, calls=%fused_computation.6.clone.1 | convolution fusion | flops 136577024 | bytes 5373953 | tf_op jit(solution)/shard_map/while/body/eval_jaxpr/dot_general | solution.py:88
  103.5 2.7 %fusion.72 = (f32[2048]{0:T(1024)S(1)}, f32[512,2048]{1,0:T(8,128)}) fusion(bf16[2048,64]{1,0:T(8,128)(2,1)S(1)} %get-tuple-element.147, bf16[512,128]{1,0:T(8,128)(2,1)S(1)} %dynamic-slice_bitcast_fusion.2), kind=kOutput, calls=%fused_computation.4.clone.1 | convolution fusion | flops 136312832 | bytes 4595712 | tf_op jit(solution)/shard_map/while/body/eval_jaxpr/qd,kd->qk/dot_general | solution.py:84
  106.2 3.1 %convolution_add_fusion.2 = f32[2048,64]{0,1:T(8,128)S(1)} fusion(f32[512,2048]{1,0:T(8,128)} %get-tuple-element.127, f32[2048,64]{0,1:T(8,128)S(1)} %get-tuple-element.137, pred[]{:T(512)S(6)} %compare.19, bf16[512,128]{1,0:T(8,128)(2,1)S(1)} %dynamic-slice_bitcast_fusion.2), kind=kOutput, calls=%fused_computation.6.clone.1 | convolution fusion | flops 136577024 | bytes 5373953 | tf_op jit(solution)/shard_map/while/body/eval_jaxpr/dot_general | solution.py:88
  109.3 2.7 %fusion.72 = (f32[2048]{0:T(1024)S(1)}, f32[512,2048]{1,0:T(8,128)}) fusion(bf16[2048,64]{1,0:T(8,128)(2,1)S(1)} %get-tuple-element.147, bf16[512,128]{1,0:T(8,128)(2,1)S(1)} %dynamic-slice_bitcast_fusion.2), kind=kOutput, calls=%fused_computation.4.clone.1 | convolution fusion | flops 136312832 | bytes 4595712 | tf_op jit(solution)/shard_map/while/body/eval_jaxpr/qd,kd->qk/dot_general | solution.py:84
  112.0 3.1 %convolution_add_fusion.2 = f32[2048,64]{0,1:T(8,128)S(1)} fusion(f32[512,2048]{1,0:T(8,128)} %get-tuple-element.127, f32[2048,64]{0,1:T(8,128)S(1)} %get-tuple-element.137, pred[]{:T(512)S(6)} %compare.19, bf16[512,128]{1,0:T(8,128)(2,1)S(1)} %dynamic-slice_bitcast_fusion.2), kind=kOutput, calls=%fused_computation.6.clone.1 | convolution fusion | flops 136577024 | bytes 5373953 | tf_op jit(solution)/shard_map/while/body/eval_jaxpr/dot_general | solution.py:88
  115.1 2.7 %fusion.72 = (f32[2048]{0:T(1024)S(1)}, f32[512,2048]{1,0:T(8,128)}) fusion(bf16[2048,64]{1,0:T(8,128)(2,1)S(1)} %get-tuple-element.147, bf16[512,128]{1,0:T(8,128)(2,1)S(1)} %dynamic-slice_bitcast_fusion.2), kind=kOutput, calls=%fused_computation.4.clone.1 | convolution fusion | flops 136312832 | bytes 4595712 | tf_op jit(solution)/shard_map/while/body/eval_jaxpr/qd,kd->qk/dot_general | solution.py:84
  117.8 3.1 %convolution_add_fusion.2 = f32[2048,64]{0,1:T(8,128)S(1)} fusion(f32[512,2048]{1,0:T(8,128)} %get-tuple-element.127, f32[2048,64]{0,1:T(8,128)S(1)} %get-tuple-element.137, pred[]{:T(512)S(6)} %compare.19, bf16[512,128]{1,0:T(8,128)(2,1)S(1)} %dynamic-slice_bitcast_fusion.2), kind=kOutput, calls=%fused_computation.6.clone.1 | convolution fusion | flops 136577024 | bytes 5373953 | tf_op jit(solution)/shard_map/while/body/eval_jaxpr/dot_general | solution.py:88
  120.9 2.7 %fusion.72 = (f32[2048]{0:T(1024)S(1)}, f32[512,2048]{1,0:T(8,128)}) fusion(bf16[2048,64]{1,0:T(8,128)(2,1)S(1)} %get-tuple-element.147, bf16[512,128]{1,0:T(8,128)(2,1)S(1)} %dynamic-slice_bitcast_fusion.2), kind=kOutput, calls=%fused_computation.4.clone.1 | convolution fusion | flops 136312832 | bytes 4595712 | tf_op jit(solution)/shard_map/while/body/eval_jaxpr/qd,kd->qk/dot_general | solution.py:84
  123.6 3.1 %convolution_add_fusion.2 = f32[2048,64]{0,1:T(8,128)S(1)} fusion(f32[512,2048]{1,0:T(8,128)} %get-tuple-element.127, f32[2048,64]{0,1:T(8,128)S(1)} %get-tuple-element.137, pred[]{:T(512)S(6)} %compare.19, bf16[512,128]{1,0:T(8,128)(2,1)S(1)} %dynamic-slice_bitcast_fusion.2), kind=kOutput, calls=%fused_computation.6.clone.1 | convolution fusion | flops 136577024 | bytes 5373953 | tf_op jit(solution)/shard_map/while/body/eval_jaxpr/dot_general | solution.py:88
  126.7 2.7 %fusion.72 = (f32[2048]{0:T(1024)S(1)}, f32[512,2048]{1,0:T(8,128)}) fusion(bf16[2048,64]{1,0:T(8,128)(2,1)S(1)} %get-tuple-element.147, bf16[512,128]{1,0:T(8,128)(2,1)S(1)} %dynamic-slice_bitcast_fusion.2), kind=kOutput, calls=%fused_computation.4.clone.1 | convolution fusion | flops 136312832 | bytes 4595712 | tf_op jit(solution)/shard_map/while/body/eval_jaxpr/qd,kd->qk/dot_general | solution.py:84
  129.4 3.1 %convolution_add_fusion.2 = f32[2048,64]{0,1:T(8,128)S(1)} fusion(f32[512,2048]{1,0:T(8,128)} %get-tuple-element.127, f32[2048,64]{0,1:T(8,128)S(1)} %get-tuple-element.137, pred[]{:T(512)S(6)} %compare.19, bf16[512,128]{1,0:T(8,128)(2,1)S(1)} %dynamic-slice_bitcast_fusion.2), kind=kOutput, calls=%fused_computation.6.clone.1 | convolution fusion | flops 136577024 | bytes 5373953 | tf_op jit(solution)/shard_map/while/body/eval_jaxpr/dot_general | solution.py:88
  132.5 2.7 %fusion.72 = (f32[2048]{0:T(1024)S(1)}, f32[512,2048]{1,0:T(8,128)}) fusion(bf16[2048,64]{1,0:T(8,128)(2,1)S(1)} %get-tuple-element.147, bf16[512,128]{1,0:T(8,128)(2,1)S(1)} %dynamic-slice_bitcast_fusion.2), kind=kOutput, calls=%fused_computation.4.clone.1 | convolution fusion | flops 136312832 | bytes 4595712 | tf_op jit(solution)/shard_map/while/body/eval_jaxpr/qd,kd->qk/dot_general | solution.py:84
  135.2 3.1 %convolution_add_fusion.2 = f32[2048,64]{0,1:T(8,128)S(1)} fusion(f32[512,2048]{1,0:T(8,128)} %get-tuple-element.127, f32[2048,64]{0,1:T(8,128)S(1)} %get-tuple-element.137, pred[]{:T(512)S(6)} %compare.19, bf16[512,128]{1,0:T(8,128)(2,1)S(1)} %dynamic-slice_bitcast_fusion.2), kind=kOutput, calls=%fused_computation.6.clone.1 | convolution fusion | flops 136577024 | bytes 5373953 | tf_op jit(solution)/shard_map/while/body/eval_jaxpr/dot_general | solution.py:88
  138.3 0.2 reshape.365
  138.6 2.1 %convolution_convert_fusion = bf16[512,2048]{1,0:T(8,128)(2,1)} fusion(bf16[512,256]{0,1:T(8,128)(2,1)S(1)} %bitcast.57, bf16[256,2048]{1,0:T(8,128)(2,1)S(1)} %copy-done), kind=kOutput, calls=%fused_computation.20 | convolution fusion | flops 537919488 | bytes 3407872 | tf_op jit(solution)/shard_map/dot_general | solution.py:111
  140.7 0.7 copy-done.4
  141.6 5.0 %all-to-all-start.1 = ((bf16[8,48,512]{2,1,0:T(8,128)(2,1)}), bf16[8,48,512]{2,1,0:T(8,128)(2,1)S(1)}, u32[]{:S(2)}, u32[]{:S(2)}) async-start(bf16[8,48,512]{2,1,0:T(8,128)(2,1)} %reduce-scatter.5.cloned.1.call-done), calls=%async_computation.3 | async-start | bytes 786432 | tf_op jit(solution)/shard_map/all_to_all | solution.py:140
  146.6 25.8 %reduce-scatter.3.cloned.1.call-done = bf16[128,2048]{1,0:T(8,128)(2,1)} async-done(((bf16[512,2048]{1,0:T(8,128)(2,1)}), bf16[128,2048]{1,0:T(8,128)(2,1)}) %reduce-scatter.3.cloned.1.call-update) | async-done | bytes 524304 | tf_op jit(solution)/shard_map/reduce_scatter | solution.py:110
  172.4 1.2 fusion.19
  173.7 2.0 %fusion.21 = bf16[128,2048]{1,0:T(8,128)(2,1)} fusion(bf16[128,2048]{1,0:T(8,128)(2,1)} %reduce-scatter.3.cloned.1.call-done, f32[2048]{0:T(1024)S(1)} %copy-done.5, f32[128]{0:T(128)S(1)} %add_rsqrt_fusion.3), kind=kLoop, calls=%fused_computation.29 | loop fusion | flops 1048576 | bytes 1057280 | tf_op jit(solution)/shard_map/convert_element_type | solution.py:116
  175.7 1.2 gather_fusion.1
  176.8 0.3 reshape.373
  177.2 1.4 multiply_reduce_fusion
  (80 shorter events, 1.9 us)
Async XLA Ops:
  8.0 130.6 %copy-start = (bf16[256,2048]{1,0:T(8,128)(2,1)S(1)}, bf16[256,2048]{1,0:T(8,128)(2,1)}, u32[]{:S(2)}) copy-start(bf16[256,2048]{1,0:T(8,128)(2,1)} %param.21) | copy-start | bytes 3145732
  18.1 7.5 %copy-start.2 = (bf16[512,256]{1,0:T(8,128)(2,1)S(1)}, bf16[512,256]{1,0:T(8,128)(2,1)}, u32[]{:S(2)}) copy-start(bf16[512,256]{1,0:T(8,128)(2,1)} %param.18) | copy-start | bytes 786436
  18.2 7.5 %copy-start.3 = (bf16[512,256]{1,0:T(8,128)(2,1)S(1)}, bf16[512,256]{1,0:T(8,128)(2,1)}, u32[]{:S(2)}) copy-start(bf16[512,256]{1,0:T(8,128)(2,1)} %param.17) | copy-start | bytes 786436
  18.2 8.0 %copy-start.6 = (f32[64]{0:T(128)S(1)}, f32[64]{0:T(128)}, u32[]{:S(2)}) copy-start(f32[64]{0:T(128)} %param.20) | copy-start | bytes 772
  18.2 9.2 %copy-start.1 = (bf16[512,256]{1,0:T(8,128)(2,1)S(1)}, bf16[512,256]{1,0:T(8,128)(2,1)}, u32[]{:S(2)}) copy-start(bf16[512,256]{1,0:T(8,128)(2,1)} %param.16) | copy-start | bytes 786436
  18.2 62.4 %all-to-all-start = ((bf16[8,48,2048]{2,1,0:T(8,128)(2,1)}), bf16[8,48,2048]{2,1,0:T(8,128)(2,1)}, u32[]{:S(2)}, u32[]{:S(2)}) async-start(bf16[8,48,2048]{2,1,0:T(8,128)(2,1)} %bitcast.13), calls=%async_computation.1 | async-start | bytes 3145728 | tf_op jit(solution)/shard_map/all_to_all | solution.py:130
  25.6 2.3 %copy-start.7 = (f32[64]{0:T(128)S(1)}, f32[64]{0:T(128)}, u32[]{:S(2)}) copy-start(f32[64]{0:T(128)} %param.19) | copy-start | bytes 772
  25.6 53.3 %all-gather.2.cloned.1.call-start = ((), (), s32[]{:S(2)}) async-start(), calls=%async_computation.4 | async-start | bytes 1179648 | tf_op jit(solution)/shard_map/all_gather | solution.py:98
  27.2 114.3 %reduce-scatter.5.cloned.1.call-start = ((), (), s32[]{:S(2)}) async-start(), calls=%async_computation.6 | async-start | bytes 1966080 | tf_op jit(solution)/shard_map/reduce_scatter | solution.py:137
  80.6 4.6 %copy-start.8 = (bf16[1,2048,1024]{2,1,0:T(8,128)(2,1)S(1)}, bf16[1,2048,1024]{2,1,0:T(8,128)(2,1)}, u32[]{:S(2)}) copy-start(bf16[1,2048,1024]{2,1,0:T(8,128)(2,1)} %param.28) | copy-start | bytes 12582916
  85.2 3.6 %copy-start.9 = (bf16[1,1024,2048]{2,1,0:T(8,128)(2,1)S(1)}, bf16[1,1024,2048]{2,1,0:T(8,128)(2,1)}, u32[]{:S(2)}) copy-start(bf16[1,1024,2048]{2,1,0:T(8,128)(2,1)} %param.29) | copy-start | bytes 12582916
  91.8 80.6 %reduce-scatter.3.cloned.1.call-start = ((), (), s32[]{:S(2)}) async-start(), calls=%async_computation.5 | async-start | bytes 2621440 | tf_op jit(solution)/shard_map/reduce_scatter | solution.py:110
  140.7 0.7 copy-start.4
  140.7 33.0 %copy-start.5 = (f32[2048]{0:T(1024)S(1)}, f32[2048]{0:T(1024)}, u32[]{:S(2)}) copy-start(f32[2048]{0:T(1024)} %param.22) | copy-start | bytes 24580
  141.6 34.1 %all-to-all-start.1 = ((bf16[8,48,512]{2,1,0:T(8,128)(2,1)}), bf16[8,48,512]{2,1,0:T(8,128)(2,1)S(1)}, u32[]{:S(2)}, u32[]{:S(2)}) async-start(bf16[8,48,512]{2,1,0:T(8,128)(2,1)} %reduce-scatter.5.cloned.1.call-done), calls=%async_computation.3 | async-start | bytes 786432 | tf_op jit(solution)/shard_map/all_to_all | solution.py:140
Sparse Core Ops, SparseCore 0:
  29.0 49.8 all-gather.1
Sparse Core Ops, SparseCore 1:
  91.9 28.3 reduce-scatter.4
  140.8 31.6 reduce-scatter.2
where the time goes:
time: 187 us; the launch traced here: 186 us
  waiting for transfers between devices  76.5 us (41%)
  matrix products  59.2 us (32%)
  between operations  15.9 us (9%)
  starting transfers between devices  12.5 us (7%)
  local copies, waits for them, and re-layouts  11.2 us (6%)
  other arithmetic  10.4 us (6%)
    all_gather x1, waiting for transfers between devices, mixer_half(): gathered_piece = lax.all_gather(paired, 'ep', axis=0, tiled=True)  50.5 us
    reduce_scatter x1, waiting for transfers between devices, mixer_half(): lax.psum_scatter(jnp.dot(head_out, w_out, preferred_element_type=jnp.floa...  25.8 us
    dot_general x8, matrix products, attend_block(): jnp.dot(weights.astype(jnp.bfloat16), block_values, preferred_element_typ...  24.7 us
    dot_general x8, matrix products, attend_block(): jnp.einsum('qd,kd->qk', query_rows, block_keys, preferred_element_type=jn...  21.2 us
    all_to_all x1, starting transfers between devices, experts_half(): lax.all_to_all(outgoing, 'ep', split_axis=0, concat_axis=0, tiled=True)  7.42 us
    all_to_all x1, starting transfers between devices, experts_half(): lax.all_to_all(summed, 'ep', split_axis=0, concat_axis=0, tiled=True)  4.98 us
    dot_general x1, matrix products, experts_half(): gate_pre = jnp.dot(arrived, w_gate[0], preferred_element_type=jnp.float32)  4.59 us
    unnamed x26, local copies, waits for them, and re-layouts  3.79 us
  transfers between devices with their start and end apart: 5, of which 2 were waited for; matrix products, arithmetic and copies ran while one was open for 30% of the time, Pallas kernels for 0%

commit v1 on v0

--- a/solution.py
+++ b/solution.py
@@ -1,3 +1,4 @@
+import functools
 import jax
 import jax.numpy as jnp
 from jax import lax
@@ -6,6 +7,36 @@
 GRID_W = 128
 EPSILON = 1e-06
 ROPE_BASE = 10000.0
+
+
+def work_weights_on(my_data, where_dim):
+    my_data = jnp.moveaxis(my_data, 0, where_dim)
+    piece_now = my_data.shape
+    return my_data.reshape(
+        *piece_now[:where_dim],
+        piece_now[where_dim] * piece_now[where_dim + 1],
+        *piece_now[where_dim + 2 :]
+    )
+
+
+def _supply_all_chains(xin, peer_axis, axis_k):
+    world = jax.lax.axis_size(peer_axis)
+    gallery = list(map(lambda num: (num, (num + 1) % world), range(world)))
+    fields = [(k, u) for u, k in gallery]
+    top, new = ([], [])
+    for jj in range(world - 1):
+        if jj % 2 == 0:
+            top.append(jax.lax.ppermute(top[-1] if top else xin, axis_name=peer_axis, perm=gallery))
+        else:
+            new.append(jax.lax.ppermute(new[-1] if new else xin, axis_name=peer_axis, perm=fields))
+    all_values = jnp.stack([*top[::-1], xin, *new])
+    plain = jax.lax.axis_index(peer_axis)
+    item_now = plain - len(top)
+    all_values = all_values[(jnp.arange(world) - item_now) % world]
+    return work_weights_on(all_values, axis_k)
+
+
+_clear_skins = functools.partial(_supply_all_chains, peer_axis="ep", axis_k=0)
 
 
 def head_norm(values, gain):
@@ -95,7 +126,7 @@
         jnp.zeros((local_heads * row_count,), jnp.float32),
     )
     running = zero_init
-    gathered_piece = lax.all_gather(paired, "ep", axis=0, tiled=True)
+    gathered_piece = _clear_skins(paired)
     piece_rows = gathered_piece.shape[0]
     blocks = gathered_piece.reshape(piece_rows // 512, 512, gathered_piece.shape[1])
 

time: 187 us -> 226 us (1.21)
  waiting for transfers between devices: 76.5 us -> 97.5 us
  starting transfers between devices: 12.5 us -> 27.8 us
  local copies, waits for them, and re-layouts: 11.2 us -> 17.3 us
    all_gather x1 -> x0, waiting for transfers between devices: 50.5 us -> none  [mixer_half(): gathered_piece = lax.all_gather(paired, 'ep', axis=0, tiled=True)]
    ppermute x0 -> x7, waiting for transfers between devices: none -> 36.1 us  [the longest x4 36.1 us: _supply_all_chains(): jax.lax.ppermute(top[-1] if top else xin, axis_name=peer_axis, perm=gallery)]
    reduce_scatter x1, waiting for transfers between devices: 0.03 us -> 29.4 us  [experts_half(): lax.psum_scatter(partial_out.astype(jnp.bfloat16), 'tp', scatter_dimensio...]
    ppermute x0 -> x7, starting transfers between devices: none -> 17.6 us  [the longest x3 12.6 us: _supply_all_chains(): jax.lax.ppermute(new[-1] if new else xin, axis_name=peer_axis, perm=fields)]
    all_to_all x1, waiting for transfers between devices: 0.01 us -> 9.51 us  [experts_half(): lax.all_to_all(summed, 'ep', split_axis=0, concat_axis=0, tiled=True)]
    reduce_scatter x1, waiting for transfers between devices: 25.8 us -> 22.4 us  [mixer_half(): lax.psum_scatter(jnp.dot(head_out, w_out, preferred_element_type=jnp.floa...]
    all_to_all x1, starting transfers between devices: 7.42 us -> 4.42 us  [experts_half(): lax.all_to_all(outgoing, 'ep', split_axis=0, concat_axis=0, tiled=True)]
    unnamed x26 -> x29, local copies, waits for them, and re-layouts: 3.79 us -> 5.38 us
  transfers between devices with their start and end apart: 5 -> 11, of which waited for: 2 -> 6; matrix products, arithmetic and copies ran while one was open for 30% -> 35% of each run, Pallas kernels for 0% -> 0%
where the time goes in v1:
time: 226 us
  waiting for transfers between devices  97.5 us (43%)
  matrix products  59.1 us (26%)
  starting transfers between devices  27.8 us (12%)
  local copies, waits for them, and re-layouts  17.3 us (8%)
  between operations  14.5 us (6%)
  other arithmetic  8.98 us (4%)
    ppermute x4, waiting for transfers between devices, _supply_all_chains(): jax.lax.ppermute(top[-1] if top else xin, axis_name=peer_axis, perm=gallery)  36.1 us
    reduce_scatter x1, waiting for transfers between devices, experts_half(): lax.psum_scatter(partial_out.astype(jnp.bfloat16), 'tp', scatter_dimensio...  29.4 us
    dot_general x8, matrix products, attend_block(): jnp.dot(weights.astype(jnp.bfloat16), block_values, preferred_element_typ...  24.6 us
    reduce_scatter x1, waiting for transfers between devices, mixer_half(): lax.psum_scatter(jnp.dot(head_out, w_out, preferred_element_type=jnp.floa...  22.4 us
    dot_general x8, matrix products, attend_block(): jnp.einsum('qd,kd->qk', query_rows, block_keys, preferred_element_type=jn...  21.3 us
    ppermute x3, starting transfers between devices, _supply_all_chains(): jax.lax.ppermute(new[-1] if new else xin, axis_name=peer_axis, perm=fields)  12.6 us
    all_to_all x1, waiting for transfers between devices, experts_half(): lax.all_to_all(summed, 'ep', split_axis=0, concat_axis=0, tiled=True)  9.51 us
    all_to_all x1, starting transfers between devices, experts_half(): lax.all_to_all(summed, 'ep', split_axis=0, concat_axis=0, tiled=True)  5.51 us
  transfers between devices with their start and end apart: 11, of which 6 were waited for; matrix products, arithmetic and copies ran while one was open for 35% of the time, Pallas kernels for 0%

profile of v1, /device:TPU:0, one launch (start us, length us, event | category | flops | bytes accessed | tf_op | source)
XLA Modules:
  0.0 225.5 jit_solution(9066628744527531024)
XLA Ops:
  7.2 1.2 constant_dynamic-slice_fusion.1
  8.7 0.7 fusion.29
  9.8 3.0 %collective-permute-start = (bf16[512,128]{0,1:T(8,128)(2,1)S(1)}, bf16[512,128]{0,1:T(8,128)(2,1)S(1)}, u32[]{:S(2)}, u32[]{:S(2)}) collective-permute-start(bf16[512,128]{0,1:T(8,128)(2,1)S(1)} %pad_maximum_fusion), channel_id=1, source_target_pairs={{0,4},{4,8},{8,12},{12,16},{16,20},{20,24},{24,28},{28,0},{1,5},{5... | collective-permute-start | bytes 393224 | tf_op jit(solution)/shard_map/ppermute | solution.py:29
  12.9 3.1 %collective-permute-start.4 = (bf16[512,128]{0,1:T(8,128)(2,1)S(1)}, bf16[512,128]{0,1:T(8,128)(2,1)S(1)}, u32[]{:S(2)}, u32[]{:S(2)}) collective-permute-start(bf16[512,128]{0,1:T(8,128)(2,1)S(1)} %pad_maximum_fusion), channel_id=1, source_target_pairs={{4,0},{8,4},{12,8},{16,12},{20,16},{24,20},{28,24},{0,28},{5,1},{9... | collective-permute-start | bytes 393224 | tf_op jit(solution)/shard_map/ppermute | solution.py:31
  16.0 0.8 copy.40
  17.0 0.7 broadcast_multiply_fusion
  18.9 1.4 scatter_custom_fusion
  20.8 3.1 %gather_fusion.1 = bf16[384,2048]{1,0:T(8,128)(2,1)} fusion(bf16[129,2048]{1,0:T(8,128)(2,1)S(1)} %concatenate.17, s32[1024]{0:T(1024)S(1)} %pad_clamp_fusion.1), kind=kCustom, calls=%fused_computation.1 | custom fusion | bytes 3147264 | tf_op jit(solution)/shard_map/gather | solution.py:160
  24.0 4.4 %all-to-all-start = ((bf16[8,48,2048]{2,1,0:T(8,128)(2,1)}), bf16[8,48,2048]{2,1,0:T(8,128)(2,1)}, u32[]{:S(2)}, u32[]{:S(2)}) async-start(bf16[8,48,2048]{2,1,0:T(8,128)(2,1)} %bitcast.21), calls=%async_computation.1 | async-start | bytes 3145728 | tf_op jit(solution)/shard_map/all_to_all | solution.py:161
  28.8 1.9 collective-permute-start.1
  31.0 30.6 %collective-permute-done.1 = bf16[512,128]{0,1:T(8,128)(2,1)S(1)} collective-permute-done((bf16[512,128]{0,1:T(8,128)(2,1)S(1)}, bf16[512,128]{0,1:T(8,128)(2,1)S(1)}, u32[]{:S(2)}, u32[]{:S(2)}) %collective-permute-start.1) | collective-permute-done | bytes 131104 | tf_op jit(solution)/shard_map/ppermute | solution.py:29
  61.7 4.8 %collective-permute-start.5 = (bf16[512,128]{0,1:T(8,128)(2,1)S(1)}, bf16[512,128]{0,1:T(8,128)(2,1)S(1)}, u32[]{:S(2)}, u32[]{:S(2)}) collective-permute-start(bf16[512,128]{0,1:T(8,128)(2,1)S(1)} %collective-permute-done.4), channel_id=1, source_target_pairs={{4,0},{8,4},{12,8},{16,12},{20,16},{24,20},{28,24},{0,28},{5,1},{9... | collective-permute-start | bytes 393224 | tf_op jit(solution)/shard_map/ppermute | solution.py:31
  66.5 2.9 %collective-permute-done.2 = bf16[512,128]{0,1:T(8,128)(2,1)S(1)} collective-permute-done((bf16[512,128]{0,1:T(8,128)(2,1)S(1)}, bf16[512,128]{0,1:T(8,128)(2,1)S(1)}, u32[]{:S(2)}, u32[]{:S(2)}) %collective-permute-start.2) | collective-permute-done | bytes 131104 | tf_op jit(solution)/shard_map/ppermute | solution.py:29
  69.7 4.8 %collective-permute-start.6 = (bf16[512,128]{0,1:T(8,128)(2,1)S(1)}, bf16[512,128]{0,1:T(8,128)(2,1)S(1)}, u32[]{:S(2)}, u32[]{:S(2)}) collective-permute-start(bf16[512,128]{0,1:T(8,128)(2,1)S(1)} %collective-permute-done.5), channel_id=1, source_target_pairs={{4,0},{8,4},{12,8},{16,12},{20,16},{24,20},{28,24},{0,28},{5,1},{9... | collective-permute-start | bytes 393224 | tf_op jit(solution)/shard_map/ppermute | solution.py:31
  74.5 2.7 %collective-permute-done.3 = bf16[512,128]{0,1:T(8,128)(2,1)S(1)} collective-permute-done((bf16[512,128]{0,1:T(8,128)(2,1)S(1)}, bf16[512,128]{0,1:T(8,128)(2,1)S(1)}, u32[]{:S(2)}, u32[]{:S(2)}) %collective-permute-start.3) | collective-permute-done | bytes 131104 | tf_op jit(solution)/shard_map/ppermute | solution.py:29
  77.8 0.7 bitcast_dynamic-update-slice_fusion.6
  78.5 0.7 bitcast_dynamic-update-slice_fusion.5
  81.8 0.7 bitcast_dynamic-update-slice_fusion
  82.4 1.8 gather_fusion
  84.3 47.3 %while.13 = (s32[]{:T(128)}, f32[2048,64]{0,1:T(8,128)S(1)}, f32[2048]{0:T(1024)S(1)}, bf16[8,512,128]{1,2,0:T(8,128)(2,1)S(1)}, bf16[2048,64]{1,0:T(8,128)(2,1)S(1)}, /*index=5*/s32[]{:T(128)}, s32[]{:T(128)}) while((s32[]{:T(128)}, f32[2048,64]{0,1:T(8,128)S(1)}, f32[2048]{0:T(1024)S(1)}, bf16[8,512,128]{1,2,0:T(8,128)(2,1)S(1)}, ...), condition=%wide.region_4.5_spmd.clone, body=%wide.region_2.4_spmd.clone.sunk | while | flops 272893952 | bytes 10518620 | solution.py:136
  84.4 2.7 %fusion.74 = (f32[2048]{0:T(1024)S(1)}, f32[512,2048]{1,0:T(8,128)}) fusion(bf16[2048,64]{1,0:T(8,128)(2,1)S(1)} %get-tuple-element.147, bf16[512,128]{1,0:T(8,128)(2,1)S(1)} %bitcast.70), kind=kOutput, calls=%fused_computation.5.clone.1 | convolution fusion | flops 136312832 | bytes 4595712 | tf_op jit(solution)/shard_map/while/body/eval_jaxpr/qd,kd->qk/dot_general | solution.py:115
  87.1 3.1 %convolution_add_fusion.2 = f32[2048,64]{0,1:T(8,128)S(1)} fusion(f32[512,2048]{1,0:T(8,128)} %get-tuple-element.127, f32[2048,64]{0,1:T(8,128)S(1)} %get-tuple-element.137, pred[]{:T(512)S(6)} %compare.26, bf16[512,128]{1,0:T(8,128)(2,1)S(1)} %bitcast.71), kind=kOutput, calls=%fused_computation.7.clone.1 | convolution fusion | flops 136577024 | bytes 5373953 | tf_op jit(solution)/shard_map/while/body/eval_jaxpr/dot_general | solution.py:119
  90.4 2.7 %fusion.74 = (f32[2048]{0:T(1024)S(1)}, f32[512,2048]{1,0:T(8,128)}) fusion(bf16[2048,64]{1,0:T(8,128)(2,1)S(1)} %get-tuple-element.147, bf16[512,128]{1,0:T(8,128)(2,1)S(1)} %bitcast.70), kind=kOutput, calls=%fused_computation.5.clone.1 | convolution fusion | flops 136312832 | bytes 4595712 | tf_op jit(solution)/shard_map/while/body/eval_jaxpr/qd,kd->qk/dot_general | solution.py:115
  93.0 3.1 %convolution_add_fusion.2 = f32[2048,64]{0,1:T(8,128)S(1)} fusion(f32[512,2048]{1,0:T(8,128)} %get-tuple-element.127, f32[2048,64]{0,1:T(8,128)S(1)} %get-tuple-element.137, pred[]{:T(512)S(6)} %compare.26, bf16[512,128]{1,0:T(8,128)(2,1)S(1)} %bitcast.71), kind=kOutput, calls=%fused_computation.7.clone.1 | convolution fusion | flops 136577024 | bytes 5373953 | tf_op jit(solution)/shard_map/while/body/eval_jaxpr/dot_general | solution.py:119
  96.3 2.7 %fusion.74 = (f32[2048]{0:T(1024)S(1)}, f32[512,2048]{1,0:T(8,128)}) fusion(bf16[2048,64]{1,0:T(8,128)(2,1)S(1)} %get-tuple-element.147, bf16[512,128]{1,0:T(8,128)(2,1)S(1)} %bitcast.70), kind=kOutput, calls=%fused_computation.5.clone.1 | convolution fusion | flops 136312832 | bytes 4595712 | tf_op jit(solution)/shard_map/while/body/eval_jaxpr/qd,kd->qk/dot_general | solution.py:115
  98.9 3.1 %convolution_add_fusion.2 = f32[2048,64]{0,1:T(8,128)S(1)} fusion(f32[512,2048]{1,0:T(8,128)} %get-tuple-element.127, f32[2048,64]{0,1:T(8,128)S(1)} %get-tuple-element.137, pred[]{:T(512)S(6)} %compare.26, bf16[512,128]{1,0:T(8,128)(2,1)S(1)} %bitcast.71), kind=kOutput, calls=%fused_computation.7.clone.1 | convolution fusion | flops 136577024 | bytes 5373953 | tf_op jit(solution)/shard_map/while/body/eval_jaxpr/dot_general | solution.py:119
  102.2 2.7 %fusion.74 = (f32[2048]{0:T(1024)S(1)}, f32[512,2048]{1,0:T(8,128)}) fusion(bf16[2048,64]{1,0:T(8,128)(2,1)S(1)} %get-tuple-element.147, bf16[512,128]{1,0:T(8,128)(2,1)S(1)} %bitcast.70), kind=kOutput, calls=%fused_computation.5.clone.1 | convolution fusion | flops 136312832 | bytes 4595712 | tf_op jit(solution)/shard_map/while/body/eval_jaxpr/qd,kd->qk/dot_general | solution.py:115
  104.9 3.1 %convolution_add_fusion.2 = f32[2048,64]{0,1:T(8,128)S(1)} fusion(f32[512,2048]{1,0:T(8,128)} %get-tuple-element.127, f32[2048,64]{0,1:T(8,128)S(1)} %get-tuple-element.137, pred[]{:T(512)S(6)} %compare.26, bf16[512,128]{1,0:T(8,128)(2,1)S(1)} %bitcast.71), kind=kOutput, calls=%fused_computation.7.clone.1 | convolution fusion | flops 136577024 | bytes 5373953 | tf_op jit(solution)/shard_map/while/body/eval_jaxpr/dot_general | solution.py:119
  108.1 2.7 %fusion.74 = (f32[2048]{0:T(1024)S(1)}, f32[512,2048]{1,0:T(8,128)}) fusion(bf16[2048,64]{1,0:T(8,128)(2,1)S(1)} %get-tuple-element.147, bf16[512,128]{1,0:T(8,128)(2,1)S(1)} %bitcast.70), kind=kOutput, calls=%fused_computation.5.clone.1 | convolution fusion | flops 136312832 | bytes 4595712 | tf_op jit(solution)/shard_map/while/body/eval_jaxpr/qd,kd->qk/dot_general | solution.py:115
  110.8 3.1 %convolution_add_fusion.2 = f32[2048,64]{0,1:T(8,128)S(1)} fusion(f32[512,2048]{1,0:T(8,128)} %get-tuple-element.127, f32[2048,64]{0,1:T(8,128)S(1)} %get-tuple-element.137, pred[]{:T(512)S(6)} %compare.26, bf16[512,128]{1,0:T(8,128)(2,1)S(1)} %bitcast.71), kind=kOutput, calls=%fused_computation.7.clone.1 | convolution fusion | flops 136577024 | bytes 5373953 | tf_op jit(solution)/shard_map/while/body/eval_jaxpr/dot_general | solution.py:119
  114.0 2.7 %fusion.74 = (f32[2048]{0:T(1024)S(1)}, f32[512,2048]{1,0:T(8,128)}) fusion(bf16[2048,64]{1,0:T(8,128)(2,1)S(1)} %get-tuple-element.147, bf16[512,128]{1,0:T(8,128)(2,1)S(1)} %bitcast.70), kind=kOutput, calls=%fused_computation.5.clone.1 | convolution fusion | flops 136312832 | bytes 4595712 | tf_op jit(solution)/shard_map/while/body/eval_jaxpr/qd,kd->qk/dot_general | solution.py:115
  116.7 3.1 %convolution_add_fusion.2 = f32[2048,64]{0,1:T(8,128)S(1)} fusion(f32[512,2048]{1,0:T(8,128)} %get-tuple-element.127, f32[2048,64]{0,1:T(8,128)S(1)} %get-tuple-element.137, pred[]{:T(512)S(6)} %compare.26, bf16[512,128]{1,0:T(8,128)(2,1)S(1)} %bitcast.71), kind=kOutput, calls=%fused_computation.7.clone.1 | convolution fusion | flops 136577024 | bytes 5373953 | tf_op jit(solution)/shard_map/while/body/eval_jaxpr/dot_general | solution.py:119
  120.0 2.7 %fusion.74 = (f32[2048]{0:T(1024)S(1)}, f32[512,2048]{1,0:T(8,128)}) fusion(bf16[2048,64]{1,0:T(8,128)(2,1)S(1)} %get-tuple-element.147, bf16[512,128]{1,0:T(8,128)(2,1)S(1)} %bitcast.70), kind=kOutput, calls=%fused_computation.5.clone.1 | convolution fusion | flops 136312832 | bytes 4595712 | tf_op jit(solution)/shard_map/while/body/eval_jaxpr/qd,kd->qk/dot_general | solution.py:115
  122.6 3.1 %convolution_add_fusion.2 = f32[2048,64]{0,1:T(8,128)S(1)} fusion(f32[512,2048]{1,0:T(8,128)} %get-tuple-element.127, f32[2048,64]{0,1:T(8,128)S(1)} %get-tuple-element.137, pred[]{:T(512)S(6)} %compare.26, bf16[512,128]{1,0:T(8,128)(2,1)S(1)} %bitcast.71), kind=kOutput, calls=%fused_computation.7.clone.1 | convolution fusion | flops 136577024 | bytes 5373953 | tf_op jit(solution)/shard_map/while/body/eval_jaxpr/dot_general | solution.py:119
  125.9 2.7 %fusion.74 = (f32[2048]{0:T(1024)S(1)}, f32[512,2048]{1,0:T(8,128)}) fusion(bf16[2048,64]{1,0:T(8,128)(2,1)S(1)} %get-tuple-element.147, bf16[512,128]{1,0:T(8,128)(2,1)S(1)} %bitcast.70), kind=kOutput, calls=%fused_computation.5.clone.1 | convolution fusion | flops 136312832 | bytes 4595712 | tf_op jit(solution)/shard_map/while/body/eval_jaxpr/qd,kd->qk/dot_general | solution.py:115
  128.5 3.1 %convolution_add_fusion.2 = f32[2048,64]{0,1:T(8,128)S(1)} fusion(f32[512,2048]{1,0:T(8,128)} %get-tuple-element.127, f32[2048,64]{0,1:T(8,128)S(1)} %get-tuple-element.137, pred[]{:T(512)S(6)} %compare.26, bf16[512,128]{1,0:T(8,128)(2,1)S(1)} %bitcast.71), kind=kOutput, calls=%fused_computation.7.clone.1 | convolution fusion | flops 136577024 | bytes 5373953 | tf_op jit(solution)/shard_map/while/body/eval_jaxpr/dot_general | solution.py:119
  131.9 2.1 convolution_convert_fusion
  134.3 4.6 %fusion.12 = f32[384,1024]{1,0:T(8,128)S(1)} fusion(bf16[384,2048]{1,0:T(8,128)(2,1)} %bitcast.22, bf16[1,2048,1024]{2,1,0:T(8,128)(2,1)} %param.27), kind=kOutput, calls=%fused_computation.19 | convolution fusion | flops 1610612736 | bytes 7340032 | tf_op jit(solution)/shard_map/dot_general | solution.py:163
  138.9 3.5 %multiply_convert_fusion = bf16[384,1024]{1,0:T(8,128)(2,1)S(1)} fusion(f32[384,1024]{1,0:T(8,128)S(1)} %fusion.12, bf16[384,2048]{1,0:T(8,128)(2,1)} %bitcast.22, bf16[1,2048,1024]{2,1,0:T(8,128)(2,1)S(1)} %copy-done.7), kind=kOutput, calls=%fused_computation.23 | convolution fusion | flops 1612972032 | bytes 8126464 | tf_op jit(solution)/shard_map/dot_general | solution.py:164
  142.5 3.0 %fusion.14 = bf16[8,48,2048]{2,1,0:T(8,128)(2,1)} fusion(bf16[8,48,1024]{2,1,0:T(8,128)(2,1)S(1)} %bitcast.79, bf16[1,1024,2048]{2,1,0:T(8,128)(2,1)S(1)} %copy-done.8), kind=kOutput, calls=%fused_computation.22 | convolution fusion | flops 1611399168 | bytes 6553600 | tf_op jit(solution)/shard_map/dot_general | solution.py:166
  145.7 22.4 %reduce-scatter.3.cloned.1.call-done = bf16[128,2048]{1,0:T(8,128)(2,1)} async-done(((bf16[512,2048]{1,0:T(8,128)(2,1)}), bf16[128,2048]{1,0:T(8,128)(2,1)}) %reduce-scatter.3.cloned.1.call-update) | async-done | bytes 524304 | tf_op jit(solution)/shard_map/reduce_scatter | solution.py:141
  168.1 1.2 fusion.19
  169.4 29.4 %reduce-scatter.5.cloned.1.call-done = bf16[8,48,512]{2,1,0:T(8,128)(2,1)} async-done(((bf16[8,48,2048]{2,1,0:T(8,128)(2,1)}), bf16[8,48,512]{2,1,0:T(8,128)(2,1)}) %reduce-scatter.5.cloned.1.call-update) | async-done | bytes 393232 | tf_op jit(solution)/shard_map/reduce_scatter | solution.py:168
  198.8 5.5 %all-to-all-start.1 = ((bf16[8,48,512]{2,1,0:T(8,128)(2,1)}), bf16[8,48,512]{2,1,0:T(8,128)(2,1)S(1)}, u32[]{:S(2)}, u32[]{:S(2)}) async-start(bf16[8,48,512]{2,1,0:T(8,128)(2,1)} %reduce-scatter.5.cloned.1.call-done), calls=%async_computation.3 | async-start | bytes 786432 | tf_op jit(solution)/shard_map/all_to_all | solution.py:171
  204.3 2.0 fusion.21
  206.3 9.5 %all-to-all-done.1 = bf16[8,48,512]{2,1,0:T(8,128)(2,1)S(1)} async-done(((bf16[8,48,512]{2,1,0:T(8,128)(2,1)}), bf16[8,48,512]{2,1,0:T(8,128)(2,1)S(1)}, u32[]{:S(2)}, u32[]{:S(2)}) %all-to-all-start.1) | async-done | bytes 393248 | tf_op jit(solution)/shard_map/all_to_all | solution.py:171
  215.8 1.2 gather_fusion.2
  217.3 1.4 multiply_reduce_fusion
  (107 shorter events, 9.1 us)
Async XLA Ops:
  7.2 124.8 %copy-start = (bf16[256,2048]{1,0:T(8,128)(2,1)S(1)}, bf16[256,2048]{1,0:T(8,128)(2,1)}, u32[]{:S(2)}) copy-start(bf16[256,2048]{1,0:T(8,128)(2,1)} %param.21) | copy-start | bytes 3145732
  7.2 13.2 %copy-start.1 = (bf16[128,2048]{1,0:T(8,128)(2,1)S(1)}, bf16[128,2048]{1,0:T(8,128)(2,1)}, u32[]{:S(2)}) copy-start(bf16[128,2048]{1,0:T(8,128)(2,1)} %param.23) | copy-start | bytes 1572868
  7.2 13.4 %copy-start.4 = (f32[2048]{0:T(1024)S(1)}, f32[2048]{0:T(1024)}, u32[]{:S(2)}) copy-start(f32[2048]{0:T(1024)} %param.26) | copy-start | bytes 24580
  9.8 19.0 %collective-permute-start = (bf16[512,128]{0,1:T(8,128)(2,1)S(1)}, bf16[512,128]{0,1:T(8,128)(2,1)S(1)}, u32[]{:S(2)}, u32[]{:S(2)}) collective-permute-start(bf16[512,128]{0,1:T(8,128)(2,1)S(1)} %pad_maximum_fusion), channel_id=1, source_target_pairs={{0,4},{4,8},{8,12},{12,16},{16,20},{20,24},{24,28},{28,0},{1,5},{5... | collective-permute-start | bytes 393224 | tf_op jit(solution)/shard_map/ppermute | solution.py:29
  12.9 48.9 %collective-permute-start.4 = (bf16[512,128]{0,1:T(8,128)(2,1)S(1)}, bf16[512,128]{0,1:T(8,128)(2,1)S(1)}, u32[]{:S(2)}, u32[]{:S(2)}) collective-permute-start(bf16[512,128]{0,1:T(8,128)(2,1)S(1)} %pad_maximum_fusion), channel_id=1, source_target_pairs={{4,0},{8,4},{12,8},{16,12},{20,16},{24,20},{28,24},{0,28},{5,1},{9... | collective-permute-start | bytes 393224 | tf_op jit(solution)/shard_map/ppermute | solution.py:31
  24.0 4.5 %copy-start.2 = (bf16[512,256]{1,0:T(8,128)(2,1)S(1)}, bf16[512,256]{1,0:T(8,128)(2,1)}, u32[]{:S(2)}) copy-start(bf16[512,256]{1,0:T(8,128)(2,1)} %param.16) | copy-start | bytes 786436
  24.0 4.7 %copy-start.6 = (f32[64]{0:T(128)S(1)}, f32[64]{0:T(128)}, u32[]{:S(2)}) copy-start(f32[64]{0:T(128)} %param.19) | copy-start | bytes 772
  24.0 110.3 %all-to-all-start = ((bf16[8,48,2048]{2,1,0:T(8,128)(2,1)}), bf16[8,48,2048]{2,1,0:T(8,128)(2,1)}, u32[]{:S(2)}, u32[]{:S(2)}) async-start(bf16[8,48,2048]{2,1,0:T(8,128)(2,1)} %bitcast.21), calls=%async_computation.1 | async-start | bytes 3145728 | tf_op jit(solution)/shard_map/all_to_all | solution.py:161
  28.4 139.8 %reduce-scatter.3.cloned.1.call-start = ((), (), s32[]{:S(2)}) async-start(), calls=%async_computation.4 | async-start | bytes 2621440 | tf_op jit(solution)/shard_map/reduce_scatter | solution.py:141
  28.8 32.8 %collective-permute-start.1 = (bf16[512,128]{0,1:T(8,128)(2,1)S(1)}, bf16[512,128]{0,1:T(8,128)(2,1)S(1)}, u32[]{:S(2)}, u32[]{:S(2)}) collective-permute-start(bf16[512,128]{0,1:T(8,128)(2,1)S(1)} %collective-permute-done), channel_id=1, source_target_pairs={{0,4},{4,8},{8,12},{12,16},{16,20},{20,24},{24,28},{28,0},{1,5},{5... | collective-permute-start | bytes 393224 | tf_op jit(solution)/shard_map/ppermute | solution.py:29
  61.6 7.8 %collective-permute-start.2 = (bf16[512,128]{0,1:T(8,128)(2,1)S(1)}, bf16[512,128]{0,1:T(8,128)(2,1)S(1)}, u32[]{:S(2)}, u32[]{:S(2)}) collective-permute-start(bf16[512,128]{0,1:T(8,128)(2,1)S(1)} %collective-permute-done.1), channel_id=1, source_target_pairs={{0,4},{4,8},{8,12},{12,16},{16,20},{20,24},{24,28},{28,0},{1,5},{5... | collective-permute-start | bytes 393224 | tf_op jit(solution)/shard_map/ppermute | solution.py:29
  61.7 8.0 %collective-permute-start.5 = (bf16[512,128]{0,1:T(8,128)(2,1)S(1)}, bf16[512,128]{0,1:T(8,128)(2,1)S(1)}, u32[]{:S(2)}, u32[]{:S(2)}) collective-permute-start(bf16[512,128]{0,1:T(8,128)(2,1)S(1)} %collective-permute-done.4), channel_id=1, source_target_pairs={{4,0},{8,4},{12,8},{16,12},{20,16},{24,20},{28,24},{0,28},{5,1},{9... | collective-permute-start | bytes 393224 | tf_op jit(solution)/shard_map/ppermute | solution.py:31
  69.4 7.8 %collective-permute-start.3 = (bf16[512,128]{0,1:T(8,128)(2,1)S(1)}, bf16[512,128]{0,1:T(8,128)(2,1)S(1)}, u32[]{:S(2)}, u32[]{:S(2)}) collective-permute-start(bf16[512,128]{0,1:T(8,128)(2,1)S(1)} %collective-permute-done.2), channel_id=1, source_target_pairs={{0,4},{4,8},{8,12},{12,16},{16,20},{20,24},{24,28},{28,0},{1,5},{5... | collective-permute-start | bytes 393224 | tf_op jit(solution)/shard_map/ppermute | solution.py:29
  69.7 12.0 %collective-permute-start.6 = (bf16[512,128]{0,1:T(8,128)(2,1)S(1)}, bf16[512,128]{0,1:T(8,128)(2,1)S(1)}, u32[]{:S(2)}, u32[]{:S(2)}) collective-permute-start(bf16[512,128]{0,1:T(8,128)(2,1)S(1)} %collective-permute-done.5), channel_id=1, source_target_pairs={{4,0},{8,4},{12,8},{16,12},{20,16},{24,20},{28,24},{0,28},{5,1},{9... | collective-permute-start | bytes 393224 | tf_op jit(solution)/shard_map/ppermute | solution.py:31
  134.1 64.7 %reduce-scatter.5.cloned.1.call-start = ((), (), s32[]{:S(2)}) async-start(), calls=%async_computation.5 | async-start | bytes 1966080 | tf_op jit(solution)/shard_map/reduce_scatter | solution.py:168
  134.3 4.6 %copy-start.7 = (bf16[1,2048,1024]{2,1,0:T(8,128)(2,1)S(1)}, bf16[1,2048,1024]{2,1,0:T(8,128)(2,1)}, u32[]{:S(2)}) copy-start(bf16[1,2048,1024]{2,1,0:T(8,128)(2,1)} %param.28) | copy-start | bytes 12582916
  138.9 3.6 %copy-start.8 = (bf16[1,1024,2048]{2,1,0:T(8,128)(2,1)S(1)}, bf16[1,1024,2048]{2,1,0:T(8,128)(2,1)}, u32[]{:S(2)}) copy-start(bf16[1,1024,2048]{2,1,0:T(8,128)(2,1)} %param.29) | copy-start | bytes 12582916
  142.5 3.0 %copy-start.3 = (f32[128,2]{0,1:T(2,128)S(1)}, f32[128,2]{0,1:T(2,128)}, u32[]{:S(2)}) copy-start(f32[128,2]{0,1:T(2,128)} %param.25) | copy-start | bytes 3076
  145.5 58.8 %copy-start.5 = (f32[2048]{0:T(1024)S(1)}, f32[2048]{0:T(1024)}, u32[]{:S(2)}) copy-start(f32[2048]{0:T(1024)} %param.22) | copy-start | bytes 24580
  198.8 17.1 %all-to-all-start.1 = ((bf16[8,48,512]{2,1,0:T(8,128)(2,1)}), bf16[8,48,512]{2,1,0:T(8,128)(2,1)S(1)}, u32[]{:S(2)}, u32[]{:S(2)}) async-start(bf16[8,48,512]{2,1,0:T(8,128)(2,1)} %reduce-scatter.5.cloned.1.call-done), calls=%async_computation.3 | async-start | bytes 786432 | tf_op jit(solution)/shard_map/all_to_all | solution.py:171
Sparse Core Ops, SparseCore 0:
  134.2 33.9 reduce-scatter.2
  170.7 28.0 reduce-scatter.4
